TPU v7x, 512 devices: a whole 4x4x16 slice. The times are simulated.
512 devices in a mesh: sp: 16 (over y, x), tp: 32 (over z, core).
Axes of the slice: x: 4, y: 4, z: 16, core: 2. Of those that a mesh axis runs over, the one named last changes fastest.
Arguments:
- stream: bfloat16 [8192, 4096], P('sp', 'tp'), may hold values from -6 to 6
- gain_first: bfloat16 [4096], P('tp'), may hold values from 0.099609375 to 1.8984375
- query_first: bfloat16 [4096, 4096], P('sp', 'tp'), may hold values from -0.09375 to 0.09375
- key_first: bfloat16 [4096, 4096], P('sp', 'tp'), may hold values from -0.09375 to 0.09375
- value_first: bfloat16 [4096, 4096], P('sp', 'tp'), may hold values from -0.09375 to 0.09375
- offset_first: float32 [32, 15, 31], P('tp'), may hold values from -4 to 254
- gain_second: bfloat16 [4096], P('tp'), may hold values from 0.099609375 to 1.8984375
- query_second: bfloat16 [4096, 4096], P('sp', 'tp'), may hold values from -0.09375 to 0.09375
- key_second: bfloat16 [4096, 4096], P('sp', 'tp'), may hold values from -0.09375 to 0.09375
- value_second: bfloat16 [4096, 4096], P('sp', 'tp'), may hold values from -0.09375 to 0.09375
- offset_second: float32 [32, 15, 31], P('tp'), may hold values from -4 to 254
Outputs:
- result: bfloat16 [8192, 4096], P('sp', 'tp')
All inputs are finite; a program needn't handle non-finite values.
Results may differ from a plain program's by a relative error of at most 0.008.
Values may be sent and summed in bfloat16 or wider, within the bound.
No kernel may reach another device: no remote copies, remote signals or barrier semaphores. Data moves between devices by JAX's collectives and lax.ppermute only.
A program may use at most 64 MiB of HBM per device.

v0:
```python
import jax
import jax.numpy as jnp
import numpy as np
from jax import lax
from jax.sharding import PartitionSpec as P

GRID_W = 64
epsilon = 1e-06


def turned_gather(arrays, axis, dims):
    turned = [jnp.moveaxis(a, dim, 0) for a, dim in zip(arrays, dims)]
    both = jnp.concatenate([t.reshape(len(t), -1) for t in turned], axis=1)
    filled, at, gathered = (lax.all_gather(both, axis, axis=0, tiled=True), 0, [])
    for t, dim in zip(turned, dims):
        section = filled[:, at : at + t[0].size].reshape(-1, *t.shape[1:])
        gathered.append(jnp.moveaxis(section, 0, dim))
        at += t[0].size
    return tuple(gathered)


def padded_2(block, sides, width):
    for axis, dim in sides:
        count = lax.axis_size(axis)
        forward = [(i, i + 1) for i in range(count - 1)]
        backward = [(target, source) for source, target in forward]
        low = lax.ppermute(
            lax.slice_in_dim(block, block.shape[dim] - width, None, axis=dim), axis, forward
        )
        high = lax.ppermute(lax.slice_in_dim(block, 0, width, axis=dim), axis, backward)
        block = jnp.concatenate([low, block, high], axis=dim)
    return block


def sent_together(arrays, axis, dim, along):
    ends, at = ([], 0)
    for a in arrays[:-1]:
        at += a.shape[along]
        ends.append(at)
    both = jnp.concatenate(arrays, axis=along)
    return tuple(jnp.split(lax.all_gather(both, axis, axis=dim, tiled=True), ends, axis=along))


def attend(query, keys, values, table, row_start, total_rows):
    rows_here, width, heads, head_size = query.shape
    blocks = width // 16
    query_cols = np.arange(width).reshape(blocks, 16)
    window_start = np.clip(query_cols - 8, 0, width - 16)
    key_cols = np.clip(np.arange(blocks) * 16 - 8, 0, width - 32)[:, None] + np.arange(32)
    column_ok = (key_cols[:, None, :] >= window_start[:, :, None]) & (
        key_cols[:, None, :] < window_start[:, :, None] + 16
    )
    column_offset = np.clip(key_cols[:, None, :] - query_cols[:, :, None] + 15, 0, 30)
    column_bias = table[:, :, column_offset]
    mask = jnp.asarray(column_ok)[None, :, :, None, :]
    factor = head_size ** (-0.5)

    def one_row(index):
        grid_row = row_start + index
        first = jnp.clip(grid_row - 4, 0, total_rows - 8)
        local = first - row_start + 4
        key_block = lax.dynamic_slice_in_dim(keys, local, 8, 0)[:, key_cols]
        value_block = lax.dynamic_slice_in_dim(values, local, 8, 0)[:, key_cols]
        query_row = lax.dynamic_index_in_dim(query, index, 0, keepdims=False).reshape(
            blocks, 16, heads, head_size
        )
        scores = (
            jnp.einsum(
                "jqhe,mjkhe->hjqmk", query_row, key_block, preferred_element_type=jnp.float32
            )
            * factor
        )
        row_offset = first + jnp.arange(8, dtype=jnp.int32) - grid_row + 7
        row_bias = jnp.transpose(jnp.take(column_bias, row_offset, axis=1), (0, 2, 3, 1, 4))
        scores = jnp.where(mask, scores + row_bias, -1e30)
        weight = jax.nn.softmax(scores.reshape(heads, blocks, 16, 256), axis=-1)
        rounded = weight.astype(jnp.bfloat16).reshape(heads, blocks, 16, 8, 32)
        output = jnp.einsum(
            "hjqmk,mjkhe->jqhe", rounded, value_block, preferred_element_type=jnp.float32
        )
        return output.reshape(width, heads * head_size)

    return jax.vmap(one_row)(jnp.arange(rows_here, dtype=jnp.int32))


def layer(stream, gain, table, whole_weights):
    tokens_dev, local_width = stream.shape
    widened = stream.astype(jnp.float32)
    full_rows, full_gain = turned_gather((stream, gain), "tp", (1, 0))
    full_wide = full_rows.astype(jnp.float32)
    mean_square = jnp.mean(full_wide * full_wide, axis=-1, keepdims=True)
    normed = (full_wide * lax.rsqrt(mean_square + epsilon) * full_gain.astype(jnp.float32)).astype(
        jnp.bfloat16
    )
    query = jnp.dot(normed, whole_weights[0], preferred_element_type=jnp.float32)
    key_part = jnp.dot(normed, whole_weights[1], preferred_element_type=jnp.float32)
    value_part = jnp.dot(normed, whole_weights[2], preferred_element_type=jnp.float32)
    heads_dev = table.shape[0]
    rows_dev = tokens_dev // GRID_W
    shape = (rows_dev, GRID_W, heads_dev, local_width // heads_dev)
    query = query.astype(jnp.bfloat16).reshape(shape)
    paired = jnp.stack(
        [
            key_part.astype(jnp.bfloat16).reshape(shape),
            value_part.astype(jnp.bfloat16).reshape(shape),
        ]
    )
    padded = padded_2(paired, (("sp", 1),), 4)
    row_start = lax.axis_index("sp") * rows_dev
    output = attend(query, padded[0], padded[1], table, row_start, rows_dev * lax.axis_size("sp"))
    return (widened + output.reshape(tokens_dev, local_width)).astype(jnp.bfloat16)


def body(
    stream,
    gain_first,
    query_first,
    key_first,
    value_first,
    offset_first,
    gain_second,
    query_second,
    key_second,
    value_second,
    offset_second,
):
    fetched = sent_together(
        (query_first, key_first, value_first, query_second, key_second, value_second), "sp", 0, 1
    )
    first_set = fetched[:3]
    second_set = fetched[3:]
    middle = layer(stream, gain_first, offset_first, first_set)
    return layer(middle, gain_second, offset_second, second_set)


def solution(mesh):
    placed = (
        P("sp", "tp"),
        P("tp"),
        P("sp", "tp"),
        P("sp", "tp"),
        P("sp", "tp"),
        P("tp", None, None),
        P("tp"),
        P("sp", "tp"),
        P("sp", "tp"),
        P("sp", "tp"),
        P("tp", None, None),
    )
    return jax.shard_map(body, mesh=mesh, in_specs=placed, out_specs=P("sp", "tp"), check_vma=False)
```

profile of v0, /device:TPU:6, one launch (start us, length us, event | category | flops | bytes accessed | tf_op | source)
XLA Modules:
  0.0 339.2 jit_solution(11450175371349849308)
XLA Ops:
  15.9 5.5 %gather_fusion.5 = f32[2048,15]{1,0:T(8,128)S(1)} fusion(f32[15,31]{0,1:T(8,128)S(1)} %bitcast.128, s32[2048]{0:T(1024)S(1)} %broadcast_clamp_fusion), kind=kCustom, calls=%fused_computation.7 | custom fusion | bytes 253952 | tf_op jit(solution)/shard_map/gather | solution.py:54
  24.1 70.7 %all-gather.4.cloned.1.call-done = bf16[4096,513]{0,1:T(8,128)(2,1)} async-done(((bf16[128,513]{0,1:T(8,128)(2,1)}), bf16[4096,513]{0,1:T(8,128)(2,1)}) %all-gather.4.cloned.1.call-update) | async-done | bytes 4202512 | tf_op jit(solution)/shard_map/all_gather | solution.py:14
  94.8 3.1 fusion
  98.7 5.9 %fusion.2 = bf16[4096,512]{0,1:T(8,128)(2,1)} fusion(f32[4096]{0:T(1024)S(1)} %bitcast.154, f32[512]{0:T(512)S(1)} %add_rsqrt_fusion.1, bf16[4096,513]{0,1:T(8,128)(2,1)} %all-gather.4.cloned.1.call-done), kind=kLoop, calls=%fused_computation.20 | loop fusion | flops 8388608 | bytes 8407040 | tf_op jit(solution)/shard_map/convert_element_type | solution.py:92
  104.6 65.2 %all-gather.6.cloned.1.call-done = bf16[4096,768]{1,0:T(8,128)(2,1)} async-done(((bf16[256,768]{1,0:T(8,128)(2,1)}), bf16[4096,768]{1,0:T(8,128)(2,1)}) %all-gather.6.cloned.1.call-update) | async-done | bytes 6291472 | tf_op jit(solution)/shard_map/all_gather | solution.py:41
  169.8 3.9 %convolution_convert_fusion.5 = bf16[512,128]{1,0:T(8,128)(2,1)S(1)} fusion(bf16[4096,512]{0,1:T(8,128)(2,1)} %fusion.2, bf16[4096,768]{1,0:T(8,128)(2,1)} %all-gather.6.cloned.1.call-done), kind=kOutput, calls=%fused_computation.53 | convolution fusion | flops 536936448 | bytes 5373952 | tf_op jit(solution)/shard_map/dot_general | solution.py:96
  173.7 2.5 convolution_convert_fusion.4
  176.2 3.3 collective-permute-start
  179.5 2.7 collective-permute-start.1
  182.3 2.5 convolution_convert_fusion.3
  185.3 3.2 collective-permute-done.1
  191.6 2.6 gather_fusion.4
  194.1 2.6 gather_fusion.1
  196.7 5.2 %fusion.41 = (f32[8,4,16]{2,1,0:T(4,128)S(1)}, f32[8,1,4,16,8,32]{5,3,4,2,0,1:T(8,128)S(1)}) fusion(f32[8,1,8,4,16,32]{5,4,3,2,0,1:T(8,128)} %bitcast.132, pred[8,8]{1,0:T(8,128)(4,1)S(1)} %compare_and_fusion, bf16[8,4,16,128,1]{3,2,4,1,0:T(8,128)(2,1)S(1)} %bitcast.142, bf16[4,32,8,8,128]{4,3,2,1,0:T(8,128)(2,1)} %bitcast.135, ...), kind=kOutput, calls=%fused_computation.105 | convolution fusion | flops 34209280 | bytes 3280960 | tf_op jit(solution)/shard_map/vmap(jqhe,mjkhe->hjqmk)/dot_general | solution.py:68
  206.3 5.6 %gather_fusion.11 = f32[2048,15]{1,0:T(8,128)S(1)} fusion(f32[15,31]{0,1:T(8,128)S(1)} %bitcast.129, s32[2048]{0:T(1024)S(1)} %broadcast_clamp_fusion), kind=kCustom, calls=%fused_computation.13 | custom fusion | bytes 253952 | tf_op jit(solution)/shard_map/gather | solution.py:54
  213.3 74.9 %all-gather.8.cloned.1.call-done = bf16[4096,513]{0,1:T(8,128)(2,1)} async-done(((bf16[128,513]{0,1:T(8,128)(2,1)}), bf16[4096,513]{0,1:T(8,128)(2,1)}) %all-gather.8.cloned.1.call-update) | async-done | bytes 4202512 | tf_op jit(solution)/shard_map/all_gather | solution.py:14
  288.1 3.2 fusion.3
  292.2 4.0 %fusion.5 = bf16[4096,512]{0,1:T(8,128)(2,1)S(1)} fusion(f32[4096]{0:T(1024)S(1)} %bitcast.155, f32[512]{0:T(512)S(1)} %add_rsqrt_fusion, bf16[4096,513]{0,1:T(8,128)(2,1)} %all-gather.8.cloned.1.call-done), kind=kLoop, calls=%fused_computation.23 | loop fusion | flops 8388608 | bytes 8407040 | tf_op jit(solution)/shard_map/convert_element_type | solution.py:92
  298.8 3.4 collective-permute-start.2
  302.2 2.7 collective-permute-start.3
  307.4 4.1 %collective-permute-done.3 = bf16[2,4,64,1,128]{4,2,1,3,0:T(8,128)(2,1)S(1)} collective-permute-done((bf16[2,4,64,1,128]{4,2,1,3,0:T(8,128)(2,1)S(1)}, bf16[2,4,64,1,128]{4,2,1,3,0:T(8,128)(2,1)S(1)}, u32[]{:S(2)}, u32[]{:S(2)}) %collective-permute-start.3) | collective-permute-done | bytes 131104 | tf_op jit(solution)/shard_map/ppermute | solution.py:30
  315.2 2.5 gather_fusion.10
  321.4 2.5 gather_fusion.7
  323.9 4.5 %fusion.42 = (f32[8,4,16]{2,1,0:T(4,128)S(1)}, f32[8,1,4,16,8,32]{5,3,4,2,0,1:T(8,128)S(1)}) fusion(f32[8,1,8,4,16,32]{5,4,3,2,0,1:T(8,128)S(1)} %bitcast.133, pred[8,8]{1,0:T(8,128)(4,1)S(1)} %copy-done.9, bf16[8,4,16,128,1]{3,2,4,1,0:T(8,128)(2,1)S(1)} %bitcast.141, bf16[4,32,8,8,128]{4,3,2,1,0:T(8,128)(2,1)} %bitcast.134, ...), kind=kOutput, calls=%fused_computation.106 | convolution fusion | flops 34209280 | bytes 3280960 | tf_op jit(solution)/shard_map/vmap(jqhe,mjkhe->hjqmk)/dot_general | solution.py:68
  (91 shorter events, 39.6 us)
Async XLA Ops:
  6.5 88.3 %all-gather.4.cloned.1.call-start = ((), (), s32[]{:S(2)}) async-start(), calls=%async_computation | async-start | bytes 4392960 | tf_op jit(solution)/shard_map/all_gather | solution.py:14
  8.2 161.6 %all-gather.6.cloned.1.call-start = ((), (), s32[]{:S(2)}) async-start(), calls=%async_computation.1 | async-start | bytes 6684672 | tf_op jit(solution)/shard_map/all_gather | solution.py:41
  13.4 0.7 copy-start.3
  14.2 274.0 %all-gather.8.cloned.1.call-start = ((), (), s32[]{:S(2)}) async-start(), calls=%async_computation.2 | async-start | bytes 4392960 | tf_op jit(solution)/shard_map/all_gather | solution.py:14
  22.0 2.0 copy-start.12
  24.1 172.6 %copy-start.8 = (pred[8,8]{1,0:T(8,128)(4,1)}, pred[8,8]{1,0:T(8,128)(4,1)S(1)}, u32[]{:S(2)}) copy-start(pred[8,8]{1,0:T(8,128)(4,1)S(1)} %compare_and_fusion) | copy-start | bytes 196
  169.8 3.9 %copy-start = (bf16[4096,512]{0,1:T(8,128)(2,1)S(1)}, bf16[4096,512]{0,1:T(8,128)(2,1)}, u32[]{:S(2)}) copy-start(bf16[4096,512]{0,1:T(8,128)(2,1)} %fusion.2) | copy-start | bytes 12582916
  176.2 9.1 %collective-permute-start = (bf16[2,4,64,1,128]{4,2,1,3,0:T(8,128)(2,1)S(1)}, bf16[2,4,64,1,128]{4,2,1,3,0:T(8,128)(2,1)S(1)}, u32[]{:S(2)}, u32[]{:S(2)}) collective-permute-start(bf16[2,4,64,1,128]{4,2,1,3,0:T(8,128)(2,1)S(1)} %get-tuple-element.12), channel_id=1, source_target_pairs={{0,32},{32,64},{64,96},{96,128},{128,160},{160,192},{192,224},{224... | collective-permute-start | bytes 393224 | tf_op jit(solution)/shard_map/ppermute | solution.py:27
  179.5 9.0 %collective-permute-start.1 = (bf16[2,4,64,1,128]{4,2,1,3,0:T(8,128)(2,1)S(1)}, bf16[2,4,64,1,128]{4,2,1,3,0:T(8,128)(2,1)S(1)}, u32[]{:S(2)}, u32[]{:S(2)}) collective-permute-start(bf16[2,4,64,1,128]{4,2,1,3,0:T(8,128)(2,1)S(1)} %get-tuple-element.13), channel_id=1, source_target_pairs={{32,0},{64,32},{96,64},{128,96},{160,128},{192,160},{224,192},{256... | collective-permute-start | bytes 393224 | tf_op jit(solution)/shard_map/ppermute | solution.py:30
  194.1 2.6 copy-start.6
  201.9 1.6 copy-start.2
  203.5 2.0 copy-start.5
  203.5 2.0 copy-start.11
  203.5 2.7 copy-start.10
  288.1 8.1 %slice-start = ((s8[6291456]{0:T(1024)(128)(4,1)}), s8[4194304]{0:T(1024)(128)(4,1)S(1)}, s32[]{:S(2)}) async-start(s8[6291456]{0:T(1024)(128)(4,1)} %bitcast.158), calls=%async_computation.3 | async-start | bytes 8388608
  292.2 4.0 %slice-start.1 = ((s8[6291456]{0:T(1024)(128)(4,1)}), s8[2097152]{0:T(1024)(128)(4,1)S(1)}, s32[]{:S(2)}) async-start(s8[6291456]{0:T(1024)(128)(4,1)} %bitcast.158), calls=%async_computation.4 | async-start | bytes 4194304
  298.8 8.6 %collective-permute-start.2 = (bf16[2,4,64,1,128]{4,2,1,3,0:T(8,128)(2,1)S(1)}, bf16[2,4,64,1,128]{4,2,1,3,0:T(8,128)(2,1)S(1)}, u32[]{:S(2)}, u32[]{:S(2)}) collective-permute-start(bf16[2,4,64,1,128]{4,2,1,3,0:T(8,128)(2,1)S(1)} %get-tuple-element.10), channel_id=1, source_target_pairs={{0,32},{32,64},{64,96},{96,128},{128,160},{160,192},{192,224},{224... | collective-permute-start | bytes 393224 | tf_op jit(solution)/shard_map/ppermute | solution.py:27
  302.2 9.4 %collective-permute-start.3 = (bf16[2,4,64,1,128]{4,2,1,3,0:T(8,128)(2,1)S(1)}, bf16[2,4,64,1,128]{4,2,1,3,0:T(8,128)(2,1)S(1)}, u32[]{:S(2)}, u32[]{:S(2)}) collective-permute-start(bf16[2,4,64,1,128]{4,2,1,3,0:T(8,128)(2,1)S(1)} %get-tuple-element.11), channel_id=1, source_target_pairs={{32,0},{64,32},{96,64},{128,96},{160,128},{192,160},{224,192},{256... | collective-permute-start | bytes 393224 | tf_op jit(solution)/shard_map/ppermute | solution.py:30
  321.3 2.6 copy-start.4
  321.3 2.5 copy-start.7
  321.3 2.5 copy-start.9
  328.4 1.6 copy-start.1
Sparse Core Ops, SparseCore 0:
  9.4 85.3 all-gather.3
  97.8 71.9 all-gather.5
  206.4 81.7 all-gather.7
where the time goes:
time: 340 us; the launch traced here: 339 us
  waiting for transfers between devices  218 us (64%)
  local copies, waits for them, and re-layouts  46.2 us (14%)
  matrix products  26.2 us (8%)
  other arithmetic  23.1 us (7%)
  between operations  13.5 us (4%)
  starting transfers between devices  12.2 us (4%)
    all_gather x2, waiting for transfers between devices, turned_gather(): lax.all_gather(both, axis, axis=0, tiled=True)  146 us
    all_gather x1, waiting for transfers between devices, sent_together(): lax.all_gather(both, axis, axis=dim, tiled=True)  65.2 us
    gather x4, local copies, waits for them, and re-layouts, attend(): column_bias = table[:, :, column_offset]  12.3 us
    gather x6, local copies, waits for them, and re-layouts, one_row(): key_block = lax.dynamic_slice_in_dim(keys, local, 8, 0)[:, key_cols]  10.2 us
    gather x6, local copies, waits for them, and re-layouts, one_row(): value_block = lax.dynamic_slice_in_dim(values, local, 8, 0)[:, key_cols]  10.1 us
    convert_element_type x2, other arithmetic, layer(): (full_wide * lax.rsqrt(mean_square + epsilon) * full_gain.astype(jnp.floa...  9.88 us
    dot_general x2, matrix products, one_row(): jnp.einsum('jqhe,mjkhe->hjqmk', query_row, key_block, preferred_element_t...  9.71 us
    unnamed x37, local copies, waits for them, and re-layouts  8.13 us
  transfers between devices with their start and end apart: 7, of which 5 were waited for; matrix products, arithmetic and copies ran while one was open for 11% of the time, Pallas kernels for 0%

commit v1 on v0

--- a/solution.py
+++ b/solution.py
@@ -11,7 +11,19 @@
 def turned_gather(arrays, axis, dims):
     turned = [jnp.moveaxis(a, dim, 0) for a, dim in zip(arrays, dims)]
     both = jnp.concatenate([t.reshape(len(t), -1) for t in turned], axis=1)
-    filled, at, gathered = (lax.all_gather(both, axis, axis=0, tiled=True), 0, [])
+    filled, at, gathered = (
+        jnp.concatenate(
+            lax.all_to_all(
+                jnp.stack([both for _ in range(lax.axis_size(axis))], 0),
+                axis,
+                split_axis=0,
+                concat_axis=0,
+            ),
+            0,
+        ),
+        0,
+        [],
+    )
     for t, dim in zip(turned, dims):
         section = filled[:, at : at + t[0].size].reshape(-1, *t.shape[1:])
         gathered.append(jnp.moveaxis(section, 0, dim))

time: 340 us -> 535 us (1.57)
  the two profiles are of different devices: /device:TPU:6 before, /device:TPU:46 now
where the time goes in v1:
time: 535 us; the launch traced here: 525 us
  waiting for transfers between devices  374 us (70%)
  local copies, waits for them, and re-layouts  65.3 us (12%)
  starting transfers between devices  32.9 us (6%)
  matrix products  26.5 us (5%)
  between operations  14.2 us (3%)
  other arithmetic  12.3 us (2%)
    all_to_all x2, waiting for transfers between devices, turned_gather(): lax.all_to_all(jnp.stack([both for _ in range(lax.axis_size(axis))], 0),...  368 us
    all_to_all x2, starting transfers between devices, turned_gather(): lax.all_to_all(jnp.stack([both for _ in range(lax.axis_size(axis))], 0),...  20.5 us
    gather x6, local copies, waits for them, and re-layouts, one_row(): key_block = lax.dynamic_slice_in_dim(keys, local, 8, 0)[:, key_cols]  12.4 us
    gather x6, local copies, waits for them, and re-layouts, one_row(): value_block = lax.dynamic_slice_in_dim(values, local, 8, 0)[:, key_cols]  12.3 us
    gather x4, local copies, waits for them, and re-layouts, attend(): column_bias = table[:, :, column_offset]  12.1 us
    unnamed x53, local copies, waits for them, and re-layouts  11.5 us
  transfers between devices with their start and end apart: 7, of which 4 were waited for; matrix products, arithmetic and copies ran while one was open for 6% of the time, Pallas kernels for 0%

profile of v1, /device:TPU:46, one launch (start us, length us, event | category | flops | bytes accessed | tf_op | source)
XLA Modules:
  0.0 525.1 jit_solution(4771322932335678813)
XLA Ops:
  7.5 2.6 stack.8
  10.1 15.5 %all-to-all-start = ((bf16[32,128,513]{1,2,0:T(8,128)(2,1)}), bf16[32,128,513]{1,2,0:T(8,128)(2,1)}, u32[]{:S(2)}, u32[]{:S(2)}) async-start(bf16[32,128,513]{1,2,0:T(8,128)(2,1)} %stack.8), calls=%async_computation | async-start | bytes 8519680 | tf_op jit(solution)/shard_map/all_to_all | solution.py:16
  27.0 5.5 %gather_fusion.5 = f32[2048,15]{1,0:T(8,128)S(1)} fusion(f32[15,31]{0,1:T(8,128)S(1)} %bitcast.142, s32[2048]{0:T(1024)S(1)} %broadcast_clamp_fusion), kind=kCustom, calls=%fused_computation.7 | custom fusion | bytes 253952 | tf_op jit(solution)/shard_map/gather | solution.py:66
  35.1 183.5 %all-to-all-done = bf16[32,128,513]{1,2,0:T(8,128)(2,1)} async-done(((bf16[32,128,513]{1,2,0:T(8,128)(2,1)}), bf16[32,128,513]{1,2,0:T(8,128)(2,1)}, u32[]{:S(2)}, u32[]{:S(2)}) %all-to-all-start) | async-done | bytes 4202528 | tf_op jit(solution)/shard_map/all_to_all | solution.py:16
  218.6 2.8 copy.135
  222.1 4.2 copy.100
  227.3 3.7 fusion.2
  231.0 3.9 convolution_convert_fusion.5
  237.4 3.4 collective-permute-start
  240.8 2.9 collective-permute-start.1
  246.8 3.0 collective-permute-done.1
  253.5 2.7 gather_fusion.4
  256.2 4.5 fusion.39
  266.7 2.6 gather_fusion.1
  271.8 2.6 stack.10
  274.4 4.9 all-to-all-start.1
  279.4 5.5 %gather_fusion.11 = f32[2048,15]{1,0:T(8,128)S(1)} fusion(f32[15,31]{0,1:T(8,128)S(1)} %bitcast.143, s32[2048]{0:T(1024)S(1)} %broadcast_clamp_fusion), kind=kCustom, calls=%fused_computation.13 | custom fusion | bytes 253952 | tf_op jit(solution)/shard_map/gather | solution.py:66
  286.2 184.4 %all-to-all-done.1 = bf16[32,128,513]{1,2,0:T(8,128)(2,1)} async-done(((bf16[32,128,513]{1,2,0:T(8,128)(2,1)}), bf16[32,128,513]{1,2,0:T(8,128)(2,1)}, u32[]{:S(2)}, u32[]{:S(2)}) %all-to-all-start.1) | async-done | bytes 4202528 | tf_op jit(solution)/shard_map/all_to_all | solution.py:16
  470.6 2.8 copy.134
  474.2 4.2 copy.101
  484.1 2.6 collective-permute-start.2
  486.7 3.5 collective-permute-start.3
  492.7 3.0 collective-permute-done.3
  501.9 4.5 fusion.40
  (113 shorter events, 52.0 us)
Async XLA Ops:
  10.1 15.7 %copy-start.3 = (bf16[256,128]{1,0:T(8,128)(2,1)S(1)}, bf16[256,128]{1,0:T(8,128)(2,1)}, u32[]{:S(2)}) copy-start(bf16[256,128]{1,0:T(8,128)(2,1)} %param.27) | copy-start | bytes 196612
  10.1 15.7 %copy-start.4 = (bf16[256,128]{1,0:T(8,128)(2,1)S(1)}, bf16[256,128]{1,0:T(8,128)(2,1)}, u32[]{:S(2)}) copy-start(bf16[256,128]{1,0:T(8,128)(2,1)} %param.28) | copy-start | bytes 196612
  10.1 15.7 %copy-start.5 = (bf16[256,128]{1,0:T(8,128)(2,1)S(1)}, bf16[256,128]{1,0:T(8,128)(2,1)}, u32[]{:S(2)}) copy-start(bf16[256,128]{1,0:T(8,128)(2,1)} %param.29) | copy-start | bytes 196612
  10.1 15.8 %copy-start.6 = (bf16[256,128]{1,0:T(8,128)(2,1)S(1)}, bf16[256,128]{1,0:T(8,128)(2,1)}, u32[]{:S(2)}) copy-start(bf16[256,128]{1,0:T(8,128)(2,1)} %param.32) | copy-start | bytes 196612
  10.1 15.8 %copy-start.7 = (bf16[256,128]{1,0:T(8,128)(2,1)S(1)}, bf16[256,128]{1,0:T(8,128)(2,1)}, u32[]{:S(2)}) copy-start(bf16[256,128]{1,0:T(8,128)(2,1)} %param.33) | copy-start | bytes 196612
  10.1 15.8 %copy-start.8 = (bf16[256,128]{1,0:T(8,128)(2,1)S(1)}, bf16[256,128]{1,0:T(8,128)(2,1)}, u32[]{:S(2)}) copy-start(bf16[256,128]{1,0:T(8,128)(2,1)} %param.34) | copy-start | bytes 196612
  10.1 16.8 %copy-start.15 = (f32[1,15,31]{2,0,1:T(1,128)S(1)}, f32[1,15,31]{2,0,1:T(1,128)}, u32[]{:S(2)}) copy-start(f32[1,15,31]{2,0,1:T(1,128)} %param.30) | copy-start | bytes 5584
  10.1 16.9 %copy-start.14 = (s32[2048]{0:T(1024)S(1)}, s32[2048]{0:T(1024)}, u32[]{:S(2)}) copy-start(s32[2048]{0:T(1024)} %constant.254) | copy-start | bytes 24580
  10.1 208.4 %all-to-all-start = ((bf16[32,128,513]{1,2,0:T(8,128)(2,1)}), bf16[32,128,513]{1,2,0:T(8,128)(2,1)}, u32[]{:S(2)}, u32[]{:S(2)}) async-start(bf16[32,128,513]{1,2,0:T(8,128)(2,1)} %stack.8), calls=%async_computation | async-start | bytes 8519680 | tf_op jit(solution)/shard_map/all_to_all | solution.py:16
  25.7 205.3 %all-gather.2.cloned.1.call-start = ((), (), s32[]{:S(2)}) async-start(), calls=%async_computation.2 | async-start | bytes 6684672 | tf_op jit(solution)/shard_map/all_gather | solution.py:53
  27.0 6.1 %copy-start.18 = (s32[128]{0:T(128)S(1)}, s32[128]{0:T(128)}, u32[]{:S(2)}) copy-start(s32[128]{0:T(128)} %constant.240) | copy-start | bytes 1540
  231.0 3.9 copy-start
  237.4 9.4 %collective-permute-start = (bf16[2,4,64,1,128]{4,2,1,3,0:T(8,128)(2,1)S(1)}, bf16[2,4,64,1,128]{4,2,1,3,0:T(8,128)(2,1)S(1)}, u32[]{:S(2)}, u32[]{:S(2)}) collective-permute-start(bf16[2,4,64,1,128]{4,2,1,3,0:T(8,128)(2,1)S(1)} %get-tuple-element.12), channel_id=1, source_target_pairs={{0,32},{32,64},{64,96},{96,128},{128,160},{160,192},{192,224},{224... | collective-permute-start | bytes 393224 | tf_op jit(solution)/shard_map/ppermute | solution.py:39
  240.8 9.0 %collective-permute-start.1 = (bf16[2,4,64,1,128]{4,2,1,3,0:T(8,128)(2,1)S(1)}, bf16[2,4,64,1,128]{4,2,1,3,0:T(8,128)(2,1)S(1)}, u32[]{:S(2)}, u32[]{:S(2)}) collective-permute-start(bf16[2,4,64,1,128]{4,2,1,3,0:T(8,128)(2,1)S(1)} %get-tuple-element.13), channel_id=1, source_target_pairs={{32,0},{64,32},{96,64},{128,96},{160,128},{192,160},{224,192},{256... | collective-permute-start | bytes 393224 | tf_op jit(solution)/shard_map/ppermute | solution.py:42
  263.1 3.6 copy-start.9
  269.2 2.5 copy-start.17
  274.4 5.0 copy-start.16
  274.4 196.3 %all-to-all-start.1 = ((bf16[32,128,513]{1,2,0:T(8,128)(2,1)}), bf16[32,128,513]{1,2,0:T(8,128)(2,1)}, u32[]{:S(2)}, u32[]{:S(2)}) async-start(bf16[32,128,513]{1,2,0:T(8,128)(2,1)} %stack.10), calls=%async_computation.1 | async-start | bytes 8519680 | tf_op jit(solution)/shard_map/all_to_all | solution.py:16
  279.4 6.1 %copy-start.12 = (s32[1024]{0:T(1024)S(1)}, s32[1024]{0:T(1024)}, u32[]{:S(2)}) copy-start(s32[1024]{0:T(1024)} %copy-done.11) | copy-start | bytes 12292
  478.5 2.6 slice-start
  484.1 8.6 %collective-permute-start.2 = (bf16[2,4,64,1,128]{4,2,1,3,0:T(8,128)(2,1)S(1)}, bf16[2,4,64,1,128]{4,2,1,3,0:T(8,128)(2,1)S(1)}, u32[]{:S(2)}, u32[]{:S(2)}) collective-permute-start(bf16[2,4,64,1,128]{4,2,1,3,0:T(8,128)(2,1)S(1)} %get-tuple-element.10), channel_id=1, source_target_pairs={{0,32},{32,64},{64,96},{96,128},{128,160},{160,192},{192,224},{224... | collective-permute-start | bytes 393224 | tf_op jit(solution)/shard_map/ppermute | solution.py:39
  486.7 9.0 %collective-permute-start.3 = (bf16[2,4,64,1,128]{4,2,1,3,0:T(8,128)(2,1)S(1)}, bf16[2,4,64,1,128]{4,2,1,3,0:T(8,128)(2,1)S(1)}, u32[]{:S(2)}, u32[]{:S(2)}) collective-permute-start(bf16[2,4,64,1,128]{4,2,1,3,0:T(8,128)(2,1)S(1)} %get-tuple-element.11), channel_id=1, source_target_pairs={{32,0},{64,32},{96,64},{128,96},{160,128},{192,160},{224,192},{256... | collective-permute-start | bytes 393224 | tf_op jit(solution)/shard_map/ppermute | solution.py:42
  495.8 3.6 copy-start.10
  499.4 2.5 copy-start.13
  (4 other events, 6.1 us)
Sparse Core Ops, SparseCore 0:
  29.5 75.7 all-gather.1
